TPU v7x, 32 devices: a whole 2x2x4 slice. The times are simulated.
32 devices in a mesh: grp: 2 (over x), ep: 8 (over z, y), tp: 2 (over core).
Axes of the slice: x: 2, y: 2, z: 4, core: 2. Of those that a mesh axis runs over, the one named last changes fastest.
Arguments:
- tokens: bfloat16 [2048, 4096], P(('grp', 'ep')), parts along dimension 0, may hold values from -16 to 16, as said below
- norm_gain: float32 [4096], replicated, may hold values from 0.1 to 1.9
- gate_weight: bfloat16 [8, 4096, 768], P('ep', None, 'tp'), may hold values from -0.09375 to 0.09375
- up_weight: bfloat16 [8, 4096, 768], P('ep', None, 'tp'), may hold values from -0.09375 to 0.09375
- down_weight: bfloat16 [8, 768, 4096], P('ep', 'tp'), may hold values from -0.21875 to 0.21875
- chosen: int32 [16, 8, 20], P(('grp', 'ep')), parts along dimension 0, may hold values from 0 to 128, as said below
- affinity: float32 [16, 8, 20], P(('grp', 'ep')), parts along dimension 0, may hold values from 0.2 to 1
Outputs:
- mixed: bfloat16 [2048, 4096], P(('grp', 'ep'), 'tp'), parts along dimension 0
There are 2 independent parts, one for each index of `grp`. A program takes and returns all parts, laid end to end along the dimension named above; an argument that names none is the same for every part. Nothing has to cross between parts.
Inputs may be any that keep to these rules, and one draw needn't show every extreme that they name: `tokens`: draws differ in their scale from row to row. `chosen`: in each (block, expert) row the live entries come first and are distinct; dead entries equal 128. Every expert has exactly 128 live slots in all and at least one live slot in every block; some block gives some expert exactly 20 live slots.
All inputs are finite; a program needn't handle non-finite values.
Results may differ from a plain program's by a relative error of at most 0.0095.
Values may be sent and summed in bfloat16 or wider, within the bound.
A program may use at most 64 MiB of HBM per device.

v0:
```python
import jax
import jax.numpy as jnp
from jax import lax
from jax.sharding import PartitionSpec as P

norm_eps = 1e-06


def normalize(block, norm_gain):
    values = block.astype(jnp.float32)
    scaled = values * lax.rsqrt(jnp.mean(values * values, axis=-1, keepdims=True) + norm_eps)
    return (scaled * norm_gain).astype(jnp.bfloat16)


def shards(tokens, norm_gain, gate_weight, up_weight, down_weight, chosen, affinity):
    tok_rows = tokens.shape[0]
    model_width = tokens.shape[1]
    picked_rows = chosen[0]
    outgoing = jnp.take(tokens, picked_rows, axis=0, mode="clip")
    arrived = lax.all_to_all(outgoing, "ep", split_axis=0, concat_axis=0, tiled=True)
    arrived_rows = arrived.reshape(-1, model_width)
    arrived_rows = normalize(arrived_rows, norm_gain)
    gate_proj = jnp.dot(arrived_rows, gate_weight[0], preferred_element_type=jnp.float32)
    up_value = jnp.dot(arrived_rows, up_weight[0], preferred_element_type=jnp.float32)
    hidden = (jax.nn.silu(gate_proj) * up_value).astype(jnp.bfloat16)
    columns = down_weight[0]
    summed = lax.psum_scatter(
        lax.dot_general(
            columns, hidden, (((0,), (1,)), ((), ())), preferred_element_type=jnp.float32
        ).astype(jnp.bfloat16),
        "tp",
        scatter_dimension=0,
        tiled=True,
    )
    returned = lax.all_to_all(summed, "ep", split_axis=1, concat_axis=1, tiled=True)
    weight = jnp.where(picked_rows < tok_rows, affinity[0], 0.0).astype(jnp.bfloat16).reshape(-1)
    flat_picks = picked_rows.reshape(-1)
    matches = flat_picks[None, :] == jnp.arange(tok_rows, dtype=jnp.int32)[:, None]
    combine = jnp.where(matches, weight[None, :], jnp.zeros((), jnp.bfloat16))
    mixed = lax.dot_general(
        combine, returned, (((1,), (1,)), ((), ())), preferred_element_type=jnp.float32
    )
    return mixed.astype(jnp.bfloat16)


def solution(mesh):
    in_specs = (
        P(("grp", "ep"), None),
        P(),
        P("ep", None, "tp"),
        P("ep", None, "tp"),
        P("ep", "tp", None),
        P(("grp", "ep"), None, None),
        P(("grp", "ep"), None, None),
    )
    out_specs = P(("grp", "ep"), "tp")
    return jax.shard_map(shards, mesh=mesh, in_specs=in_specs, out_specs=out_specs, check_vma=False)
```

profile of v0, /device:TPU:0, one launch (start us, length us, event | category | flops | bytes accessed | tf_op | source)
XLA Modules:
  0.0 119.4 jit_solution(9632262665727400255)
XLA Ops:
  6.5 0.0 copy-start
  6.5 0.0 reduce-scatter.2.cloned.1.call-start
  6.5 0.9 eq.15
  7.5 5.1 %gather_fusion = bf16[160,4096]{1,0:T(8,128)(2,1)} fusion(bf16[128,4096]{1,0:T(8,128)(2,1)} %param.7, s32[1024]{0:T(1024)S(1)} %pad_clamp_fusion), kind=kCustom, calls=%fused_computation | custom fusion | bytes 2622080 | tf_op jit(solution)/shard_map/jit(_take)/gather | solution.py:19
  12.6 2.4 %reshape.50 = bf16[8,20,4096]{2,1,0:T(8,128)(2,1)} reshape(bf16[160,4096]{1,0:T(8,128)(2,1)} %gather_fusion) | data formatting | bytes 2621440 | tf_op jit(solution)/shard_map/jit(_take)/gather | solution.py:19
  15.0 0.0 copy-start.1
  15.0 44.4 %all_to_all.17 = bf16[8,20,4096]{2,1,0:T(8,128)(2,1)S(1)} all-to-all(bf16[8,20,4096]{2,1,0:T(8,128)(2,1)} %reshape.50), channel_id=1, replica_groups=mesh['grp'=2,'ep'=8,'tp'=2] {'ep'}, dimensions={0} | all-to-all | bytes 2621440 | tf_op jit(solution)/shard_map/all_to_all | solution.py:20
  59.4 0.4 fusion.1
  59.8 0.0 copy-done.1
  59.8 1.6 %fusion.3 = bf16[8,20,4096]{2,1,0:T(8,128)(2,1)} fusion(bf16[8,20,4096]{2,1,0:T(8,128)(2,1)S(1)} %all_to_all.17, f32[4096]{0:T(1024)S(1)} %copy-done.1, f32[8,20]{1,0:T(8,128)S(1)} %add_rsqrt_fusion), kind=kLoop, calls=%fused_computation.7 | loop fusion | flops 2621440 | bytes 2638464 | tf_op jit(solution)/shard_map/convert_element_type | solution.py:12
  61.5 2.4 %convert_element_type.35 = bf16[160,4096]{1,0:T(8,128)(2,1)} reshape(bf16[8,20,4096]{2,1,0:T(8,128)(2,1)} %fusion.3) | data formatting | bytes 2621440 | tf_op jit(solution)/shard_map/convert_element_type | solution.py:12
  63.8 3.1 %fusion.7 = f32[160,384]{1,0:T(8,128)S(1)} fusion(bf16[160,4096]{1,0:T(8,128)(2,1)} %convert_element_type.35, bf16[1,4096,384]{2,1,0:T(8,128)(2,1)} %param.9), kind=kOutput, calls=%fused_computation.11 | convolution fusion | flops 503316480 | bytes 4702208 | tf_op jit(solution)/shard_map/dot_general | solution.py:23
  67.0 0.0 copy-done
  67.0 5.0 %fusion = bf16[4096,160]{0,1:T(8,128)(2,1)} fusion(bf16[1,384,4096]{2,1,0:T(8,128)(2,1)S(1)} %copy-done, bf16[160,4096]{1,0:T(8,128)(2,1)} %convert_element_type.35, bf16[1,4096,384]{2,1,0:T(8,128)(2,1)} %param.10, f32[160,384]{1,0:T(8,128)S(1)} %fusion.7), kind=kOutput, calls=%fused_computation.2 | convolution fusion | flops 1007656960 | bytes 9158656 | tf_op jit(solution)/shard_map/dot_general | solution.py:28
  72.0 0.0 copy-start.2
  72.0 0.0 reduce-scatter.2.cloned.1.call-update
  72.0 7.8 %reduce-scatter.2.cloned.1.call-done = bf16[2048,160]{0,1:T(8,128)(2,1)} async-done(((bf16[4096,160]{0,1:T(8,128)(2,1)}), bf16[2048,160]{0,1:T(8,128)(2,1)}) %reduce-scatter.2.cloned.1.call-update) | async-done | bytes 655376 | tf_op jit(solution)/shard_map/reduce_scatter | solution.py:27
  79.8 2.0 %all_to_all.12 = bf16[2048,8,20]{0,2,1:T(8,128)(2,1)} reshape(bf16[2048,160]{0,1:T(8,128)(2,1)} %reduce-scatter.2.cloned.1.call-done) | data formatting | bytes 1310720 | tf_op jit(solution)/shard_map/all_to_all | solution.py:35
  81.8 5.9 %all-to-all-start.1 = ((bf16[2048,8,20]{0,2,1:T(8,128)(2,1)}), bf16[2048,8,20]{0,2,1:T(8,128)(2,1)}, u32[]{:S(2)}, u32[]{:S(2)}) async-start(bf16[2048,8,20]{0,2,1:T(8,128)(2,1)} %all_to_all.12), calls=%async_computation.2 | async-start | bytes 1572864 | tf_op jit(solution)/shard_map/all_to_all | solution.py:35
  87.7 0.0 copy-done.2
  87.7 0.1 squeeze.13
  87.8 20.5 %all-to-all-done.1 = bf16[2048,8,20]{0,2,1:T(8,128)(2,1)} async-done(((bf16[2048,8,20]{0,2,1:T(8,128)(2,1)}), bf16[2048,8,20]{0,2,1:T(8,128)(2,1)}, u32[]{:S(2)}, u32[]{:S(2)}) %all-to-all-start.1) | async-done | bytes 655392 | tf_op jit(solution)/shard_map/all_to_all | solution.py:35
  108.3 2.0 %all_to_all.14 = bf16[2048,160]{0,1:T(8,128)(2,1)} reshape(bf16[2048,8,20]{0,2,1:T(8,128)(2,1)} %all-to-all-done.1) | data formatting | bytes 1310720 | tf_op jit(solution)/shard_map/all_to_all | solution.py:35
  110.4 2.2 %convolution_convert_fusion.1 = bf16[128,2048]{1,0:T(8,128)(2,1)} fusion(bf16[2048,160]{0,1:T(8,128)(2,1)} %all_to_all.14, s32[160]{0:T(256)S(1)} %eq.15, bf16[160]{0:T(256)(128)(2,1)S(1)} %fusion.28), kind=kOutput, calls=%fused_computation.13 | convolution fusion | flops 84189184 | bytes 1180608 | tf_op jit(solution)/shard_map/dot_general | solution.py:40
  (3 shorter events, 0.0 us)
Async XLA Ops:
  6.5 60.4 %copy-start = (bf16[1,384,4096]{2,1,0:T(8,128)(2,1)S(1)}, bf16[1,384,4096]{2,1,0:T(8,128)(2,1)}, u32[]{:S(2)}) copy-start(bf16[1,384,4096]{2,1,0:T(8,128)(2,1)} %param.11) | copy-start | bytes 9437188
  6.5 73.3 %reduce-scatter.2.cloned.1.call-start = ((), (), s32[]{:S(2)}) async-start(), calls=%async_computation.3 | async-start | bytes 1966080 | tf_op jit(solution)/shard_map/reduce_scatter | solution.py:27
  15.0 44.9 %copy-start.1 = (f32[4096]{0:T(1024)S(1)}, f32[4096]{0:T(1024)}, u32[]{:S(2)}) copy-start(f32[4096]{0:T(1024)} %param.8) | copy-start | bytes 49156
  72.0 15.7 %copy-start.2 = (f32[1,8,20]{2,1,0:T(8,128)S(1)}, f32[1,8,20]{2,1,0:T(8,128)}, u32[]{:S(2)}) copy-start(f32[1,8,20]{2,1,0:T(8,128)} %param.13) | copy-start | bytes 1924
  81.8 26.5 %all-to-all-start.1 = ((bf16[2048,8,20]{0,2,1:T(8,128)(2,1)}), bf16[2048,8,20]{0,2,1:T(8,128)(2,1)}, u32[]{:S(2)}, u32[]{:S(2)}) async-start(bf16[2048,8,20]{0,2,1:T(8,128)(2,1)} %all_to_all.12), calls=%async_computation.2 | async-start | bytes 1572864 | tf_op jit(solution)/shard_map/all_to_all | solution.py:35
Sparse Core Ops, SparseCore 0:
  72.1 7.6 reduce-scatter.1
where the time goes:
time: 120 us; the launch traced here: 119 us
  blocking collectives  44.4 us (37%)
  waiting for transfers between devices  28.3 us (24%)
  local copies, waits for them, and re-layouts  14.9 us (12%)
  between operations  13.4 us (11%)
  matrix products  10.3 us (9%)
  starting transfers between devices  5.89 us (5%)
  other arithmetic  2.1 us (2%)
    all_to_all x1, blocking collectives, shards(): lax.all_to_all(outgoing, 'ep', split_axis=0, concat_axis=0, tiled=True)  44.4 us
    all_to_all x1, waiting for transfers between devices, shards(): lax.all_to_all(summed, 'ep', split_axis=1, concat_axis=1, tiled=True)  20.5 us
    reduce_scatter x1, waiting for transfers between devices, shards(): lax.psum_scatter(lax.dot_general(columns, hidden, (((0,), (1,)), ((), ())...  7.78 us
    gather x2, local copies, waits for them, and re-layouts, shards(): outgoing = jnp.take(tokens, picked_rows, axis=0, mode='clip')  7.49 us
    all_to_all x1, starting transfers between devices, shards(): lax.all_to_all(summed, 'ep', split_axis=1, concat_axis=1, tiled=True)  5.89 us
    dot_general x1, matrix products, shards(): lax.dot_general(columns, hidden, (((0,), (1,)), ((), ())), preferred_elem...  5.01 us
    all_to_all x2, local copies, waits for them, and re-layouts, shards(): lax.all_to_all(summed, 'ep', split_axis=1, concat_axis=1, tiled=True)  4.08 us
    dot_general x1, matrix products, shards(): jnp.dot(arrived_rows, gate_weight[0], preferred_element_type=jnp.float32)  3.13 us
  transfers between devices with their start and end apart: 2, of which 2 were waited for; matrix products, arithmetic and copies ran while one was open for 0% of the time, Pallas kernels for 0%

commit v1 on v0

v1 whole, which is shorter than its diff:
```python
import functools

import jax
import jax.numpy as jnp
from jax import lax
from jax.experimental import pallas as pl
from jax.experimental.pallas import tpu as pltpu
from jax.sharding import PartitionSpec as P

norm_eps = 1e-06
CHUNKS = 4
bf16, f32 = jnp.bfloat16, jnp.float32


def dot(a, b):
    return jnp.dot(a, b, preferred_element_type=f32)


def iota(shape, dim):
    return lax.broadcasted_iota(jnp.int32, shape, dim)


def kernel(n, pad, tok_hbm, gain_ref, gate_hbm, up_hbm, down_hbm, chosen_ref, aff_ref, out_ref,
           tok, gate_w, up_w, down_own, down_other, picks, arrived, hid_own, hid_other, outs, ret, acc,
           load_sem, wd_sem, pick_send, pick_recv, relay_send, relay_recv, hid_sem, ret_send, ret_recv):
    me = lax.axis_index("ep")
    h = lax.axis_index("tp")
    partner = 1 - h
    rows, width = tok.shape
    half = width // 2
    cc = half // CHUNKS
    slot = chosen_ref.shape[1]
    total = n * pad
    offsets = sorted(range(1, n), key=lambda o: (-min(o, n - o), o))

    load_tok = pltpu.make_async_copy(tok_hbm, tok, load_sem.at[0])
    load_tok.start()

    barrier = pltpu.get_barrier_semaphore()
    for o in range(1, n):
        pl.semaphore_signal(barrier, inc=1, device_id={"ep": lax.rem(me + o, n)}, device_id_type=pl.DeviceIdType.MESH)
    pl.semaphore_signal(barrier, inc=1, device_id={"tp": partner}, device_id_type=pl.DeviceIdType.MESH)

    my_cols = pl.multiple_of(h * half, half)
    partner_cols = pl.multiple_of(partner * half, half)
    load_gate = pltpu.make_async_copy(gate_hbm.at[0], gate_w, load_sem.at[1])
    load_up = pltpu.make_async_copy(up_hbm.at[0], up_w, load_sem.at[2])
    load_down = pltpu.make_async_copy(down_hbm.at[0, :, pl.ds(my_cols, half)], down_own, load_sem.at[3])
    load_gate.start()
    load_up.start()
    load_down.start()

    picked = chosen_ref[...].astype(f32)
    owner = iota((total, n), 0)
    first = iota((total, n), 1) * pad
    spread = jnp.where((owner >= first) & (owner < first + pad), 1.0, 0.0).astype(bf16)
    wide = dot(spread, picked.astype(bf16))
    within = lax.rem(iota((total, slot), 0), pad) == iota((total, slot), 1)
    column = jnp.sum(jnp.where(within, wide + 1.0, 0.0), axis=1, keepdims=True) - 1.0
    select = jnp.where(iota((total, rows), 1).astype(f32) == column, 1.0, 0.0).astype(bf16)

    load_tok.wait()
    squares = jnp.zeros((rows, 1), f32)
    for i in range(8):
        piece = tok[:, i * (width // 8):(i + 1) * (width // 8)].astype(f32)
        squares = squares + jnp.sum(piece * piece, axis=1, keepdims=True)
    scale = lax.rsqrt(squares / width + norm_eps)

    pl.semaphore_wait(barrier, n)

    def pick_copy(c, dest, src):
        return pltpu.make_async_remote_copy(
            picks.at[c, dest], arrived.at[0, c, src], pick_send.at[c, dest], pick_recv.at[c, src],
            device_id={"ep": dest}, device_id_type=pl.DeviceIdType.MESH)

    def relay_copy(c, src, source):
        return pltpu.make_async_remote_copy(
            source, arrived.at[1, c, src], relay_send.at[c, src], relay_recv.at[c, src],
            device_id={"tp": partner}, device_id_type=pl.DeviceIdType.MESH)

    for c in range(CHUNKS):
        cols = pl.ds(pl.multiple_of(h * half + c * cc, cc), cc)
        normed = (tok[:, cols].astype(f32) * scale * gain_ref[:, cols]).astype(bf16)
        picks[c] = dot(select, normed).astype(bf16).reshape(n, pad, cc)
        for o in offsets:
            dest = lax.rem(me + o, n)
            pick_copy(c, dest, me).start()
        arrived[0, c, pl.ds(me, 1)] = picks[c, pl.ds(me, 1)]
        relay_copy(c, me, picks.at[c, me]).start()

    send_down = pltpu.make_async_remote_copy(
        down_hbm.at[0, :, pl.ds(partner_cols, half)], down_other, wd_sem.at[0], wd_sem.at[1],
        device_id={"tp": partner}, device_id_type=pl.DeviceIdType.MESH)
    send_down.start()

    place = jnp.where(lax.rem(iota((slot, total), 1), pad) == iota((slot, total), 0), 1.0, 0.0).astype(bf16)
    lane = iota((n, total), 1)
    low = iota((n, total), 0) * pad
    mine = (lane >= low) & (lane < low + pad)
    pick_row = jnp.sum(jnp.where(mine, dot(picked.astype(bf16), place), 0.0), axis=0, keepdims=True)
    filled = lax.rem(iota((1, total), 1), pad) < slot
    pick_row = jnp.where(filled, pick_row, -1.0)
    aff_row = jnp.sum(jnp.where(mine, dot(aff_ref[...].astype(bf16), place), 0.0), axis=0, keepdims=True)
    combine = jnp.where(iota((rows, total), 0).astype(f32) == pick_row, aff_row, 0.0).astype(bf16)

    load_gate.wait()
    load_up.wait()
    for c in range(CHUNKS):
        for o in offsets:
            src = lax.rem(me + n - o, n)
            pick_copy(c, src, src).wait_recv()
            relay_copy(c, src, arrived.at[0, c, src]).start()
        for side in range(2):
            if side == 1:
                relay_copy(c, me, picks.at[c, me]).wait_recv()
                for o in offsets:
                    src = lax.rem(me + n - o, n)
                    relay_copy(c, src, arrived.at[0, c, src]).wait_recv()
            base = h if side == 0 else partner
            depth = pl.ds(pl.multiple_of(base * half + c * cc, cc), cc)
            x = arrived[side, c].reshape(total, cc)
            g = dot(x, gate_w[depth, :])
            u = dot(x, up_w[depth, :])
            if c == 0 and side == 0:
                acc[0] = g
                acc[1] = u
            else:
                acc[0] += g
                acc[1] += u
    g = acc[0]
    hid_own[...] = (g / (1.0 + jnp.exp(-g)) * acc[1]).astype(bf16)
    send_hid = pltpu.make_async_remote_copy(
        hid_own, hid_other, hid_sem.at[0], hid_sem.at[1],
        device_id={"tp": partner}, device_id_type=pl.DeviceIdType.MESH)
    send_hid.start()

    def ret_copy(c, dest, src):
        return pltpu.make_async_remote_copy(
            outs.at[c, dest], ret.at[c, src], ret_send.at[c, dest], ret_recv.at[c, src],
            device_id={"ep": dest}, device_id_type=pl.DeviceIdType.MESH)

    load_down.wait()
    for c in range(CHUNKS):
        part = dot(hid_own[...], down_own[:, c * cc:(c + 1) * cc])
        if c == 0:
            send_down.wait_recv()
            send_hid.wait_recv()
        part = part + dot(hid_other[...], down_other[:, c * cc:(c + 1) * cc])
        outs[c] = part.astype(bf16).reshape(n, pad, cc)
        for o in offsets:
            ret_copy(c, lax.rem(me + o, n), me).start()
        ret[c, pl.ds(me, 1)] = outs[c, pl.ds(me, 1)]

    for c in range(CHUNKS):
        for o in offsets:
            src = lax.rem(me + n - o, n)
            ret_copy(c, src, src).wait_recv()
        out_ref[:, c * cc:(c + 1) * cc] = dot(combine, ret[c].reshape(total, cc)).astype(bf16)

    send_down.wait_send()
    send_hid.wait_send()
    for c in range(CHUNKS):
        relay_copy(c, me, picks.at[c, me]).wait_send()
        for o in offsets:
            src = lax.rem(me + n - o, n)
            relay_copy(c, src, arrived.at[0, c, src]).wait_send()
            dest = lax.rem(me + o, n)
            pick_copy(c, dest, me).wait_send()
            ret_copy(c, dest, me).wait_send()


def solution(mesh):
    n = mesh.shape["ep"]

    def shards(tokens, norm_gain, gate_weight, up_weight, down_weight, chosen, affinity):
        rows, width = tokens.shape
        ff = gate_weight.shape[2]
        slot = chosen.shape[2]
        pad = -(-slot // 8) * 8
        half = width // 2
        cc = half // CHUNKS
        any_spec = pl.BlockSpec(memory_space=pl.ANY)
        vmem = pl.BlockSpec(memory_space=pltpu.VMEM)
        dma = pltpu.SemaphoreType.DMA
        return pl.pallas_call(
            functools.partial(kernel, n, pad),
            out_shape=jax.ShapeDtypeStruct((rows, half), bf16),
            in_specs=[any_spec, vmem, any_spec, any_spec, any_spec, vmem, vmem],
            out_specs=vmem,
            scratch_shapes=[
                pltpu.VMEM((rows, width), bf16),
                pltpu.VMEM((width, ff), bf16),
                pltpu.VMEM((width, ff), bf16),
                pltpu.VMEM((ff, half), bf16),
                pltpu.VMEM((ff, half), bf16),
                pltpu.VMEM((CHUNKS, n, pad, cc), bf16),
                pltpu.VMEM((2, CHUNKS, n, pad, cc), bf16),
                pltpu.VMEM((n * pad, ff), bf16),
                pltpu.VMEM((n * pad, ff), bf16),
                pltpu.VMEM((CHUNKS, n, pad, cc), bf16),
                pltpu.VMEM((CHUNKS, n, pad, cc), bf16),
                pltpu.VMEM((2, n * pad, ff), f32),
                dma((4,)),
                dma((2,)),
                dma((CHUNKS, n)),
                dma((CHUNKS, n)),
                dma((CHUNKS, n)),
                dma((CHUNKS, n)),
                dma((2,)),
                dma((CHUNKS, n)),
                dma((CHUNKS, n)),
            ],
            compiler_params=pltpu.CompilerParams(
                collective_id=0, has_side_effects=True, vmem_limit_bytes=56 * 1024 * 1024
            ),
        )(tokens, norm_gain.reshape(1, -1), gate_weight, up_weight, down_weight, chosen[0], affinity[0])

    in_specs = (
        P(("grp", "ep"), None),
        P(),
        P("ep", None, "tp"),
        P("ep", None, "tp"),
        P("ep", "tp", None),
        P(("grp", "ep"), None, None),
        P(("grp", "ep"), None, None),
    )
    out_specs = P(("grp", "ep"), "tp")
    return jax.shard_map(shards, mesh=mesh, in_specs=in_specs, out_specs=out_specs, check_vma=False)
```

time: 120 us -> 51.9 us (0.43)
  Pallas kernels: 0 us -> 49.8 us
  blocking collectives: 44.4 us -> 0 us
  waiting for transfers between devices: 28.3 us -> 0 us
  between operations: 13.4 us -> 0.01 us
  local copies, waits for them, and re-layouts: 14.9 us -> 1.88 us
  matrix products: 10.3 us -> 0 us
  starting transfers between devices: 5.89 us -> 0 us
  other arithmetic: 2.1 us -> 0 us
    pallas_call x0 -> x1, Pallas kernels: none -> 49.8 us  [shards(): pl.pallas_call(functools.partial(kernel, n, pad), out_shape=jax.ShapeDtyp...]
    all_to_all x1 -> x0, blocking collectives: 44.4 us -> none  [shards(): lax.all_to_all(outgoing, 'ep', split_axis=0, concat_axis=0, tiled=True)]
    all_to_all x1 -> x0, waiting for transfers between devices: 20.5 us -> none  [shards(): lax.all_to_all(summed, 'ep', split_axis=1, concat_axis=1, tiled=True)]
    dot_general x3 -> x0, matrix products: 10.3 us -> none  [the longest x1 5.01 us: shards(): lax.dot_general(columns, hidden, (((0,), (1,)), ((), ())), preferred_elem...]
    reduce_scatter x1 -> x0, waiting for transfers between devices: 7.78 us -> none  [shards(): lax.psum_scatter(lax.dot_general(columns, hidden, (((0,), (1,)), ((), ())...]
    gather x2 -> x0, local copies, waits for them, and re-layouts: 7.49 us -> none  [shards(): outgoing = jnp.take(tokens, picked_rows, axis=0, mode='clip')]
    all_to_all x1 -> x0, starting transfers between devices: 5.89 us -> none  [shards(): lax.all_to_all(summed, 'ep', split_axis=1, concat_axis=1, tiled=True)]
    all_to_all x2 -> x0, local copies, waits for them, and re-layouts: 4.08 us -> none  [shards(): lax.all_to_all(summed, 'ep', split_axis=1, concat_axis=1, tiled=True)]
  transfers between devices with their start and end apart: 2 -> 0, of which waited for: 2 -> 0; matrix products, arithmetic and copies ran while one was open for 0% -> 0% of each run, Pallas kernels for 0% -> 0%
where the time goes in v1:
time: 51.9 us; the launch traced here: 51.7 us
  Pallas kernels  49.8 us (96%)
  local copies, waits for them, and re-layouts  1.88 us (4%)
    pallas_call x1, Pallas kernels, shards(): pl.pallas_call(functools.partial(kernel, n, pad), out_shape=jax.ShapeDtyp...  49.8 us
    unnamed x1, local copies, waits for them, and re-layouts  1.88 us

profile of v1, /device:TPU:0, one launch (start us, length us, event | category | flops | bytes accessed | tf_op | source)
XLA Modules:
  0.0 51.7 jit_solution(14630893793561529602)
XLA Ops:
  0.0 49.8 %shard_map.73 = bf16[128,2048]{1,0:T(8,128)(2,1)} custom-call(bf16[128,4096]{1,0:T(8,128)(2,1)} %tok_hbm.1, f32[1,4096]{1,0:T(1,128)} %bitcast.3, bf16[1,4096,384]{2,1,0:T(8,128)(2,1)} %gate_hbm.1, bf16[1,4096,384]{2,1,0:T(8,128)(2,1)} %up_hbm.1, bf16[1,384,4096]{2,1,0:T(8,128)(2,1)} %down_hbm.1, s32[8,20]{1,0:T(8,128)} %bitcast.4, f32[8,20]{1,0:T(8,128)} %bitcast.5), custom_call_target="tpu_custom_call" | custom-call | tf_op jit(solution)/shard_map/pallas_call | solution.py:185
  49.8 1.9 %copy.9 = bf16[128,2048]{1,0:T(8,128)(2,1)} copy(bf16[128,2048]{1,0:T(8,128)(2,1)} %shard_map.73) | data formatting | bytes 1048576

commit v2 on v0

v2 whole, which is shorter than its diff:
```python
import functools

import jax
import jax.numpy as jnp
from jax import lax
from jax.experimental import pallas as pl
from jax.experimental.pallas import tpu as pltpu
from jax.sharding import PartitionSpec as P

norm_eps = 1e-06
bf16, f32 = jnp.bfloat16, jnp.float32


def dot(a, b):
    return jnp.dot(a, b, preferred_element_type=f32)


def iota(shape, dim):
    return lax.broadcasted_iota(jnp.int32, shape, dim)


def merge(y0, y1, full):
    return jnp.concatenate(
        [y0[:, :full] + y1[:, 8:], y0[:, full:] + pltpu.roll(y1[:, :8], 4, 1)], axis=1)


def pack(y, full):
    side = y.shape[2] // 2
    y0, y1 = y[:, :, :side], y[:, :, side:]
    upper = iota((y.shape[0], 8, side), 1) < 4
    rest = jnp.where(upper, y0[:, full:], pltpu.roll(y1[:, full:], 4, 1))
    return jnp.concatenate([y0[:, :full], rest, y1[:, :full]], axis=1).astype(bf16)


def kernel(n, full, tok_hbm, gain_ref, gate_hbm, up_hbm, down_hbm, chosen_ref, aff_ref, out_ref,
           tok, gu_w, down_own, down_other, normed, picks, arrived, hid_own, hid_other, outs, ret,
           load_sem, wd_sem, pick_send, pick_recv, relay_send, relay_recv, hid_send, hid_recv, ret_send, ret_recv):
    me = lax.axis_index("ep")
    h = lax.axis_index("tp")
    partner = 1 - h
    rows, width = tok.shape
    half = width // 2
    side = half // 2
    ff = down_own.shape[0]
    slot = chosen_ref.shape[1]
    pad = full + 8
    total = n * pad
    paired = n & (n - 1) == 0
    mesh_id = pl.DeviceIdType.MESH

    def to(k):
        return me ^ k if paired else lax.rem(me + k, n)

    def back(k):
        return me ^ k if paired else lax.rem(me + n - k, n)

    place_k = (lambda e: e ^ me) if paired else (lambda e: lax.rem(e + n - me, n))
    if n >= 4:
        batches = [(n // 2, n // 2 + n // 4), (0, n // 2), (n // 2 + n // 4, n)]
        order = list(range(n // 2, n)) + list(range(1, n // 2))
    else:
        batches = [(0, n)]
        order = list(range(1, n))

    load_tok = pltpu.make_async_copy(tok_hbm, tok, load_sem.at[0])
    load_tok.start()

    barrier = pltpu.get_barrier_semaphore()
    for k in order:
        pl.semaphore_signal(barrier, inc=1, device_id={"ep": to(k)}, device_id_type=mesh_id)
    pl.semaphore_signal(barrier, inc=1, device_id={"tp": partner}, device_id_type=mesh_id)

    my_cols = pl.multiple_of(h * half, half)
    partner_cols = pl.multiple_of(partner * half, half)
    load_gate = pltpu.make_async_copy(gate_hbm.at[0], gu_w.at[:, :ff], load_sem.at[1])
    load_up = pltpu.make_async_copy(up_hbm.at[0], gu_w.at[:, ff:], load_sem.at[2])
    load_down = pltpu.make_async_copy(down_hbm.at[0, :, pl.ds(my_cols, half)], down_own, load_sem.at[3])
    load_gate.start()
    load_up.start()
    load_down.start()

    picked = chosen_ref[...].astype(f32).astype(bf16)
    row = iota((total, n), 0)
    first = place_k(iota((total, n), 1)) * pad
    spread = jnp.where((row >= first) & (row < first + pad), 1.0, 0.0).astype(bf16)
    wide = dot(spread, picked)
    within = lax.rem(iota((total, slot), 0), pad) == iota((total, slot), 1)
    column = jnp.sum(jnp.where(within, wide + 1.0, 0.0), axis=1, keepdims=True) - 1.0
    select = jnp.where(iota((total, rows), 1).astype(f32) == column, 1.0, 0.0).astype(bf16)

    load_tok.wait()
    squares = jnp.zeros((rows, 1), f32)
    for i in range(8):
        piece = tok[:, i * (width // 8):(i + 1) * (width // 8)].astype(f32)
        squares = squares + jnp.sum(piece * piece, axis=1, keepdims=True)
    scale = lax.rsqrt(squares / width + norm_eps)
    for i in range(4):
        cols = pl.ds(pl.multiple_of(h * half + i * (half // 4), half // 4), half // 4)
        normed[:, i * (half // 4):(i + 1) * (half // 4)] = (
            tok[:, cols].astype(f32) * scale * gain_ref[:, cols]).astype(bf16)

    def pick_copy(k):
        return pltpu.make_async_remote_copy(
            picks.at[k], arrived.at[0, k], pick_send.at[k], pick_recv.at[k],
            device_id={"ep": to(k)}, device_id_type=mesh_id)

    def relay_copy(k):
        source = picks.at[0] if k == 0 else arrived.at[0, k]
        return pltpu.make_async_remote_copy(
            source, arrived.at[1, k], relay_send.at[k], relay_recv.at[k],
            device_id={"tp": partner}, device_id_type=mesh_id)

    def hid_copy(i):
        span = pl.ds(batches[i][0] * pad, (batches[i][1] - batches[i][0]) * pad)
        return pltpu.make_async_remote_copy(
            hid_own.at[span], hid_other.at[span], hid_send.at[i], hid_recv.at[i],
            device_id={"tp": partner}, device_id_type=mesh_id)

    def ret_copy(k):
        return pltpu.make_async_remote_copy(
            outs.at[k], ret.at[k], ret_send.at[k], ret_recv.at[k],
            device_id={"ep": back(k)}, device_id_type=mesh_id)

    for i, (lo, hi) in enumerate(sorted(batches, key=lambda b: b[0] == 0)):
        taken = dot(select[lo * pad:hi * pad], normed[...])
        picks[lo:hi] = pack(taken.reshape(hi - lo, pad, half), full)
        if i == 0:
            pl.semaphore_wait(barrier, n)
        for k in range(max(lo, 1), hi):
            pick_copy(k).start()
    arrived[0, 0] = picks[0]
    relay_copy(0).start()

    send_down = pltpu.make_async_remote_copy(
        down_hbm.at[0, :, pl.ds(partner_cols, half)], down_other, wd_sem.at[0], wd_sem.at[1],
        device_id={"tp": partner}, device_id_type=mesh_id)
    send_down.start()

    slot_low = place_k(iota((n, total), 0)) * pad
    lane = iota((n, total), 1)
    mine = (lane >= slot_low) & (lane < slot_low + pad)
    weights = aff_ref[...].astype(bf16)

    def combine_of(second):
        at = lax.rem(iota((slot, total), 1), pad)
        if second:
            at = jnp.where(at < 4, -1, jnp.where(at < 8, at + (full - 4), at - 8))
        place = jnp.where(at == iota((slot, total), 0), 1.0, 0.0).astype(bf16)
        row_of = jnp.sum(jnp.where(mine, dot(picked, place), 0.0), axis=0, keepdims=True)
        filled = jnp.sum(place.astype(f32), axis=0, keepdims=True)
        row_of = jnp.where(filled > 0.5, row_of, -1.0)
        value = jnp.sum(jnp.where(mine, dot(weights, place), 0.0), axis=0, keepdims=True)
        return jnp.where(iota((rows, total), 0).astype(f32) == row_of, value, 0.0).astype(bf16)

    combine = [combine_of(False), combine_of(True)]

    load_gate.wait()
    load_up.wait()
    for i, (lo, hi) in enumerate(batches):
        count = hi - lo
        for k in range(max(lo, 1), hi):
            pick_copy(k).wait_recv()
            relay_copy(k).start()
        y0, y1 = None, None
        for s, base in ((0, h), (1, partner)):
            if s == 1:
                for k in range(lo, hi):
                    relay_copy(k).wait_recv()
            x0 = arrived[s, lo:hi, :pad].reshape(count * pad, side)
            x1 = arrived[s, lo:hi, full:].reshape(count * pad, side)
            p0 = dot(x0, gu_w[pl.ds(pl.multiple_of(base * half, side), side), :])
            p1 = dot(x1, gu_w[pl.ds(pl.multiple_of(base * half + side, side), side), :])
            y0, y1 = (p0, p1) if s == 0 else (y0 + p0, y1 + p1)
        y = merge(y0.reshape(count, pad, 2 * ff), y1.reshape(count, pad, 2 * ff), full).reshape(count * pad, 2 * ff)
        g = y[:, :ff]
        span = slice(lo * pad, hi * pad)
        hid_own[span] = (g / (1.0 + jnp.exp(-g)) * y[:, ff:]).astype(bf16)
        hid_copy(i).start()
        if i == 0:
            load_down.wait()
        part = dot(hid_own[span], down_own[...])
        if i == 0:
            send_down.wait_recv()
        hid_copy(i).wait_recv()
        part = part + dot(hid_other[span], down_other[...])
        outs[lo:hi] = pack(part.reshape(count, pad, half), full)
        for k in range(max(lo, 1), hi):
            ret_copy(k).start()
        if lo == 0:
            ret[0] = outs[0]

    for i, (lo, hi) in enumerate(batches):
        for k in range(max(lo, 1), hi):
            ret_copy(k).wait_recv()
    out_ref[:, :side] = dot(combine[0], ret[:, :pad].reshape(total, side)).astype(bf16)
    out_ref[:, side:] = dot(combine[1], ret[:, full:].reshape(total, side)).astype(bf16)

    send_down.wait_send()
    for i in range(len(batches)):
        hid_copy(i).wait_send()
    for k in range(n):
        relay_copy(k).wait_send()
        if k:
            pick_copy(k).wait_send()
            ret_copy(k).wait_send()


def solution(mesh):
    n = mesh.shape["ep"]

    def shards(tokens, norm_gain, gate_weight, up_weight, down_weight, chosen, affinity):
        rows, width = tokens.shape
        ff = gate_weight.shape[2]
        slot = chosen.shape[2]
        full = slot // 8 * 8 if 0 < slot % 8 <= 4 else -(-slot // 8) * 8
        pad = full + 8
        half = width // 2
        message = (n, 2 * full + 8, half // 2)
        any_spec = pl.BlockSpec(memory_space=pl.ANY)
        vmem = pl.BlockSpec(memory_space=pltpu.VMEM)
        dma = pltpu.SemaphoreType.DMA
        return pl.pallas_call(
            functools.partial(kernel, n, full),
            out_shape=jax.ShapeDtypeStruct((rows, half), bf16),
            in_specs=[any_spec, vmem, any_spec, any_spec, any_spec, vmem, vmem],
            out_specs=vmem,
            scratch_shapes=[
                pltpu.VMEM((rows, width), bf16),
                pltpu.VMEM((width, 2 * ff), bf16),
                pltpu.VMEM((ff, half), bf16),
                pltpu.VMEM((ff, half), bf16),
                pltpu.VMEM((rows, half), bf16),
                pltpu.VMEM(message, bf16),
                pltpu.VMEM((2,) + message, bf16),
                pltpu.VMEM((n * pad, ff), bf16),
                pltpu.VMEM((n * pad, ff), bf16),
                pltpu.VMEM(message, bf16),
                pltpu.VMEM(message, bf16),
                dma((4,)),
                dma((2,)),
                dma((n,)),
                dma((n,)),
                dma((n,)),
                dma((n,)),
                dma((3,)),
                dma((3,)),
                dma((n,)),
                dma((n,)),
            ],
            compiler_params=pltpu.CompilerParams(
                collective_id=0, has_side_effects=True, vmem_limit_bytes=56 * 1024 * 1024
            ),
        )(tokens, norm_gain.reshape(1, -1), gate_weight, up_weight, down_weight, chosen[0], affinity[0])

    in_specs = (
        P(("grp", "ep"), None),
        P(),
        P("ep", None, "tp"),
        P("ep", None, "tp"),
        P("ep", "tp", None),
        P(("grp", "ep"), None, None),
        P(("grp", "ep"), None, None),
    )
    out_specs = P(("grp", "ep"), "tp")
    return jax.shard_map(shards, mesh=mesh, in_specs=in_specs, out_specs=out_specs, check_vma=False)
```

time: 120 us -> 42.1 us (0.35)
  blocking collectives: 44.4 us -> 0 us
  Pallas kernels: 0 us -> 40 us
  waiting for transfers between devices: 28.3 us -> 0 us
  between operations: 13.4 us -> 0.01 us
  local copies, waits for them, and re-layouts: 14.9 us -> 1.88 us
  matrix products: 10.3 us -> 0 us
  starting transfers between devices: 5.89 us -> 0 us
  other arithmetic: 2.1 us -> 0 us
    all_to_all x1 -> x0, blocking collectives: 44.4 us -> none  [shards(): lax.all_to_all(outgoing, 'ep', split_axis=0, concat_axis=0, tiled=True)]
    pallas_call x0 -> x1, Pallas kernels: none -> 40 us  [shards(): pl.pallas_call(functools.partial(kernel, n, full), out_shape=jax.ShapeDty...]
    all_to_all x1 -> x0, waiting for transfers between devices: 20.5 us -> none  [shards(): lax.all_to_all(summed, 'ep', split_axis=1, concat_axis=1, tiled=True)]
    dot_general x3 -> x0, matrix products: 10.3 us -> none  [the longest x1 5.01 us: shards(): lax.dot_general(columns, hidden, (((0,), (1,)), ((), ())), preferred_elem...]
    reduce_scatter x1 -> x0, waiting for transfers between devices: 7.78 us -> none  [shards(): lax.psum_scatter(lax.dot_general(columns, hidden, (((0,), (1,)), ((), ())...]
    gather x2 -> x0, local copies, waits for them, and re-layouts: 7.49 us -> none  [shards(): outgoing = jnp.take(tokens, picked_rows, axis=0, mode='clip')]
    all_to_all x1 -> x0, starting transfers between devices: 5.89 us -> none  [shards(): lax.all_to_all(summed, 'ep', split_axis=1, concat_axis=1, tiled=True)]
    all_to_all x2 -> x0, local copies, waits for them, and re-layouts: 4.08 us -> none  [shards(): lax.all_to_all(summed, 'ep', split_axis=1, concat_axis=1, tiled=True)]
  transfers between devices with their start and end apart: 2 -> 0, of which waited for: 2 -> 0; matrix products, arithmetic and copies ran while one was open for 0% -> 0% of each run, Pallas kernels for 0% -> 0%
where the time goes in v2:
time: 42.1 us; the launch traced here: 41.9 us
  Pallas kernels  40 us (95%)
  local copies, waits for them, and re-layouts  1.88 us (4%)
    pallas_call x1, Pallas kernels, shards(): pl.pallas_call(functools.partial(kernel, n, full), out_shape=jax.ShapeDty...  40 us
    unnamed x1, local copies, waits for them, and re-layouts  1.88 us

profile of v2, /device:TPU:0, one launch (start us, length us, event | category | flops | bytes accessed | tf_op | source)
XLA Modules:
  0.0 41.9 jit_solution(17594447939436326119)
XLA Ops:
  0.0 40.0 %shard_map.73 = bf16[128,2048]{1,0:T(8,128)(2,1)} custom-call(bf16[128,4096]{1,0:T(8,128)(2,1)} %tok_hbm.1, f32[1,4096]{1,0:T(1,128)} %bitcast.3, bf16[1,4096,384]{2,1,0:T(8,128)(2,1)} %gate_hbm.1, bf16[1,4096,384]{2,1,0:T(8,128)(2,1)} %up_hbm.1, bf16[1,384,4096]{2,1,0:T(8,128)(2,1)} %down_hbm.1, s32[8,20]{1,0:T(8,128)} %bitcast.4, f32[8,20]{1,0:T(8,128)} %bitcast.5), custom_call_target="tpu_custom_call" | custom-call | tf_op jit(solution)/shard_map/pallas_call | solution.py:222
  40.0 1.9 %copy.9 = bf16[128,2048]{1,0:T(8,128)(2,1)} copy(bf16[128,2048]{1,0:T(8,128)(2,1)} %shard_map.73) | data formatting | bytes 1048576

commit v3 on v2

--- a/solution.py
+++ b/solution.py
@@ -32,8 +32,8 @@
     return jnp.concatenate([y0[:, :full], rest, y1[:, :full]], axis=1).astype(bf16)
 
 
-def kernel(n, full, tok_hbm, gain_ref, gate_hbm, up_hbm, down_hbm, chosen_ref, aff_ref, out_ref,
-           tok, gu_w, down_own, down_other, normed, picks, arrived, hid_own, hid_other, outs, ret,
+def kernel(n, full, tok_hbm, gain_hbm, gate_hbm, up_hbm, down_hbm, chosen_hbm, aff_hbm, out_ref,
+           tok, gain_ref, chosen_ref, aff_ref, gu_w, down_own, down_other, normed, picks, arrived, hid_own, hid_other, outs, ret,
            load_sem, wd_sem, pick_send, pick_recv, relay_send, relay_recv, hid_send, hid_recv, ret_send, ret_recv):
     me = lax.axis_index("ep")
     h = lax.axis_index("tp")
@@ -56,7 +56,7 @@
 
     place_k = (lambda e: e ^ me) if paired else (lambda e: lax.rem(e + n - me, n))
     if n >= 4:
-        batches = [(n // 2, n // 2 + n // 4), (0, n // 2), (n // 2 + n // 4, n)]
+        batches = [(0, n // 2), (n // 2, n // 2 + n // 4), (n // 2 + n // 4, n)]
         order = list(range(n // 2, n)) + list(range(1, n // 2))
     else:
         batches = [(0, n)]
@@ -64,6 +64,12 @@
 
     load_tok = pltpu.make_async_copy(tok_hbm, tok, load_sem.at[0])
     load_tok.start()
+    load_gain = pltpu.make_async_copy(gain_hbm, gain_ref, load_sem.at[4])
+    load_gain.start()
+    load_chosen = pltpu.make_async_copy(chosen_hbm, chosen_ref, load_sem.at[5])
+    load_chosen.start()
+    load_aff = pltpu.make_async_copy(aff_hbm, aff_ref, load_sem.at[6])
+    load_aff.start()
 
     barrier = pltpu.get_barrier_semaphore()
     for k in order:
@@ -79,6 +85,7 @@
     load_up.start()
     load_down.start()
 
+    load_chosen.wait()
     picked = chosen_ref[...].astype(f32).astype(bf16)
     row = iota((total, n), 0)
     first = place_k(iota((total, n), 1)) * pad
@@ -89,6 +96,7 @@
     select = jnp.where(iota((total, rows), 1).astype(f32) == column, 1.0, 0.0).astype(bf16)
 
     load_tok.wait()
+    load_gain.wait()
     squares = jnp.zeros((rows, 1), f32)
     for i in range(8):
         piece = tok[:, i * (width // 8):(i + 1) * (width // 8)].astype(f32)
@@ -121,7 +129,7 @@
             outs.at[k], ret.at[k], ret_send.at[k], ret_recv.at[k],
             device_id={"ep": back(k)}, device_id_type=mesh_id)
 
-    for i, (lo, hi) in enumerate(sorted(batches, key=lambda b: b[0] == 0)):
+    for i, (lo, hi) in enumerate([(0, n // 2), (n // 2, n // 2 + n // 4), (n // 2 + n // 4, n)]):
         taken = dot(select[lo * pad:hi * pad], normed[...])
         picks[lo:hi] = pack(taken.reshape(hi - lo, pad, half), full)
         if i == 0:
@@ -139,6 +147,7 @@
     slot_low = place_k(iota((n, total), 0)) * pad
     lane = iota((n, total), 1)
     mine = (lane >= slot_low) & (lane < slot_low + pad)
+    load_aff.wait()
     weights = aff_ref[...].astype(bf16)
 
     def combine_of(second):
@@ -222,10 +231,13 @@
         return pl.pallas_call(
             functools.partial(kernel, n, full),
             out_shape=jax.ShapeDtypeStruct((rows, half), bf16),
-            in_specs=[any_spec, vmem, any_spec, any_spec, any_spec, vmem, vmem],
+            in_specs=[any_spec] * 7,
             out_specs=vmem,
             scratch_shapes=[
                 pltpu.VMEM((rows, width), bf16),
+                pltpu.VMEM((1, width), f32),
+                pltpu.VMEM(chosen.shape[1:], jnp.int32),
+                pltpu.VMEM(affinity.shape[1:], f32),
                 pltpu.VMEM((width, 2 * ff), bf16),
                 pltpu.VMEM((ff, half), bf16),
                 pltpu.VMEM((ff, half), bf16),
@@ -236,7 +248,7 @@
                 pltpu.VMEM((n * pad, ff), bf16),
                 pltpu.VMEM(message, bf16),
                 pltpu.VMEM(message, bf16),
-                dma((4,)),
+                dma((7,)),
                 dma((2,)),
                 dma((n,)),
                 dma((n,)),

time: 42.1 us -> 38.3 us (0.910)
  the two profiles are of different devices: /device:TPU:0 before, /device:TPU:11 now
where the time goes in v3:
time: 38.3 us; the launch traced here: 38.1 us
  Pallas kernels  36.2 us (95%)
  local copies, waits for them, and re-layouts  1.88 us (5%)
    pallas_call x1, Pallas kernels, shards(): pl.pallas_call(functools.partial(kernel, n, full), out_shape=jax.ShapeDty...  36.2 us
    unnamed x1, local copies, waits for them, and re-layouts  1.88 us

profile of v3, /device:TPU:11, one launch (start us, length us, event | category | flops | bytes accessed | tf_op | source)
XLA Modules:
  0.0 38.1 jit_solution(6804500559157669662)
XLA Ops:
  0.0 36.2 %shard_map.73 = bf16[128,2048]{1,0:T(8,128)(2,1)} custom-call(bf16[128,4096]{1,0:T(8,128)(2,1)} %tok_hbm.1, f32[1,4096]{1,0:T(1,128)} %bitcast.3, bf16[1,4096,384]{2,1,0:T(8,128)(2,1)} %gate_hbm.1, bf16[1,4096,384]{2,1,0:T(8,128)(2,1)} %up_hbm.1, bf16[1,384,4096]{2,1,0:T(8,128)(2,1)} %down_hbm.1, s32[8,20]{1,0:T(8,128)} %bitcast.4, f32[8,20]{1,0:T(8,128)} %bitcast.5), custom_call_target="tpu_custom_call" | custom-call | tf_op jit(solution)/shard_map/pallas_call | solution.py:231
  36.2 1.9 %copy.9 = bf16[128,2048]{1,0:T(8,128)(2,1)} copy(bf16[128,2048]{1,0:T(8,128)(2,1)} %shard_map.73) | data formatting | bytes 1048576

commit v4 on v3

--- a/solution.py
+++ b/solution.py
@@ -32,8 +32,8 @@
     return jnp.concatenate([y0[:, :full], rest, y1[:, :full]], axis=1).astype(bf16)
 
 
-def kernel(n, full, tok_hbm, gain_hbm, gate_hbm, up_hbm, down_hbm, chosen_hbm, aff_hbm, out_ref,
-           tok, gain_ref, chosen_ref, aff_ref, gu_w, down_own, down_other, normed, picks, arrived, hid_own, hid_other, outs, ret,
+def kernel(n, full, tok_hbm, gain_hbm, gate_hbm, up_hbm, down_hbm, chosen_hbm, aff_hbm, ret, factors_hbm,
+           factors, tok, gain_ref, chosen_ref, aff_ref, gu_w, down_own, down_other, normed, picks, arrived, hid_own, hid_other, outs,
            load_sem, wd_sem, pick_send, pick_recv, relay_send, relay_recv, hid_send, hid_recv, ret_send, ret_recv):
     me = lax.axis_index("ep")
     h = lax.axis_index("tp")
@@ -134,7 +134,7 @@
         picks[lo:hi] = pack(taken.reshape(hi - lo, pad, half), full)
         if i == 0:
             pl.semaphore_wait(barrier, n)
-        for k in range(max(lo, 1), hi):
+        for k in (range(1, hi) if lo == 0 else range(hi - 1, lo - 1, -1)):
             pick_copy(k).start()
     arrived[0, 0] = picks[0]
     relay_copy(0).start()
@@ -161,7 +161,10 @@
         value = jnp.sum(jnp.where(mine, dot(weights, place), 0.0), axis=0, keepdims=True)
         return jnp.where(iota((rows, total), 0).astype(f32) == row_of, value, 0.0).astype(bf16)
 
-    combine = [combine_of(False), combine_of(True)]
+    factors[0] = combine_of(False)
+    factors[1] = combine_of(True)
+    put = pltpu.make_async_copy(factors, factors_hbm, load_sem.at[8])
+    put.start()
 
     load_gate.wait()
     load_up.wait()
@@ -196,14 +199,14 @@
         for k in range(max(lo, 1), hi):
             ret_copy(k).start()
         if lo == 0:
-            ret[0] = outs[0]
+            keep = pltpu.make_async_copy(outs.at[0], ret.at[0], load_sem.at[7])
+            keep.start()
 
     for i, (lo, hi) in enumerate(batches):
         for k in range(max(lo, 1), hi):
             ret_copy(k).wait_recv()
-    out_ref[:, :side] = dot(combine[0], ret[:, :pad].reshape(total, side)).astype(bf16)
-    out_ref[:, side:] = dot(combine[1], ret[:, full:].reshape(total, side)).astype(bf16)
-
+    keep.wait()
+    put.wait()
     send_down.wait_send()
     for i in range(len(batches)):
         hid_copy(i).wait_send()
@@ -212,6 +215,29 @@
         if k:
             pick_copy(k).wait_send()
             ret_copy(k).wait_send()
+
+
+def combine_kernel(full, ret_hbm, factors_hbm, out_hbm, ret, factors, out, sem):
+    side = ret.shape[2]
+    total = factors.shape[2]
+    pad = full + 8
+    take = [
+        pltpu.make_async_copy(factors_hbm, factors, sem.at[0]),
+        pltpu.make_async_copy(ret_hbm.at[:, :pad], ret.at[:, :pad], sem.at[1]),
+        pltpu.make_async_copy(ret_hbm.at[:, pad:], ret.at[:, pad:], sem.at[2]),
+    ]
+    put = [pltpu.make_async_copy(out.at[i], out_hbm.at[:, i * side:(i + 1) * side], sem.at[3 + i]) for i in range(2)]
+    for copy in take:
+        copy.start()
+    take[0].wait()
+    take[1].wait()
+    out[0] = dot(factors[0], ret[:, :pad].reshape(total, side)).astype(bf16)
+    put[0].start()
+    take[2].wait()
+    out[1] = dot(factors[1], ret[:, full:].reshape(total, side)).astype(bf16)
+    put[1].start()
+    put[0].wait()
+    put[1].wait()
 
 
 def solution(mesh):
@@ -226,14 +252,15 @@
         half = width // 2
         message = (n, 2 * full + 8, half // 2)
         any_spec = pl.BlockSpec(memory_space=pl.ANY)
-        vmem = pl.BlockSpec(memory_space=pltpu.VMEM)
         dma = pltpu.SemaphoreType.DMA
-        return pl.pallas_call(
+        factors = jax.ShapeDtypeStruct((2, rows, n * pad), bf16)
+        ret, factors = pl.pallas_call(
             functools.partial(kernel, n, full),
-            out_shape=jax.ShapeDtypeStruct((rows, half), bf16),
+            out_shape=(jax.ShapeDtypeStruct(message, bf16), factors),
             in_specs=[any_spec] * 7,
-            out_specs=vmem,
+            out_specs=(any_spec, any_spec),
             scratch_shapes=[
+                pltpu.VMEM((2, rows, n * pad), bf16),
                 pltpu.VMEM((rows, width), bf16),
                 pltpu.VMEM((1, width), f32),
                 pltpu.VMEM(chosen.shape[1:], jnp.int32),
@@ -247,8 +274,7 @@
                 pltpu.VMEM((n * pad, ff), bf16),
                 pltpu.VMEM((n * pad, ff), bf16),
                 pltpu.VMEM(message, bf16),
-                pltpu.VMEM(message, bf16),
-                dma((7,)),
+                dma((9,)),
                 dma((2,)),
                 dma((n,)),
                 dma((n,)),
@@ -263,6 +289,19 @@
                 collective_id=0, has_side_effects=True, vmem_limit_bytes=56 * 1024 * 1024
             ),
         )(tokens, norm_gain.reshape(1, -1), gate_weight, up_weight, down_weight, chosen[0], affinity[0])
+        return pl.pallas_call(
+            functools.partial(combine_kernel, full),
+            out_shape=jax.ShapeDtypeStruct((rows, half), bf16),
+            in_specs=[any_spec] * 2,
+            out_specs=any_spec,
+            scratch_shapes=[
+                pltpu.VMEM(message, bf16),
+                pltpu.VMEM((2, rows, n * pad), bf16),
+                pltpu.VMEM((2, rows, half // 2), bf16),
+                dma((5,)),
+            ],
+            compiler_params=pltpu.CompilerParams(vmem_limit_bytes=56 * 1024 * 1024),
+        )(ret, factors)
 
     in_specs = (
         P(("grp", "ep"), None),

time: 38.3 us -> 37.2 us (0.971)
  the two profiles are of different devices: /device:TPU:11 before, /device:TPU:16 now
where the time goes in v4:
time: 37.2 us; the launch traced here: 37.1 us
  Pallas kernels  37.1 us (100%)
    pallas_call x1, Pallas kernels, shards(): pl.pallas_call(functools.partial(kernel, n, full), out_shape=(jax.ShapeDt...  34.8 us
    pallas_call x1, Pallas kernels, shards(): pl.pallas_call(functools.partial(combine_kernel, full), out_shape=jax.Sha...  2.27 us

profile of v4, /device:TPU:16, one launch (start us, length us, event | category | flops | bytes accessed | tf_op | source)
XLA Modules:
  0.0 37.1 jit_solution(9031054420656666813)
XLA Ops:
  0.0 34.8 %shard_map.73 = (bf16[8,40,1024]{2,1,0:T(8,128)(2,1)}, bf16[2,128,192]{2,1,0:T(8,128)(2,1)}) custom-call(bf16[128,4096]{1,0:T(8,128)(2,1)} %tok_hbm.1, f32[1,4096]{1,0:T(1,128)} %bitcast.3, bf16[1,4096,384]{2,1,0:T(8,128)(2,1)} %gate_hbm.1, bf16[1,4096,384]{2,1,0:T(8,128)(2,1)} %up_hbm.1, bf16[1,384,4096]{2,1,0:T(8,128)(2,1)} %down_hbm.1, s32[8,20]{1,0:T(8,128)} %bitcast.4, ...), custom_call_target="tpu_custom_call" | custom-call | tf_op jit(solution)/shard_map/pallas_call | solution.py:257
  34.8 2.3 %shard_map.74 = bf16[128,2048]{1,0:T(8,128)(2,1)} custom-call(bf16[8,40,1024]{2,1,0:T(8,128)(2,1)} %get-tuple-element.7.ret_hbm, bf16[2,128,192]{2,1,0:T(8,128)(2,1)} %get-tuple-element.8.factors_hbm), custom_call_target="tpu_custom_call" | custom-call | tf_op jit(solution)/shard_map/pallas_call | solution.py:292

commit v5 on v4

--- a/solution.py
+++ b/solution.py
@@ -196,7 +196,7 @@
         hid_copy(i).wait_recv()
         part = part + dot(hid_other[span], down_other[...])
         outs[lo:hi] = pack(part.reshape(count, pad, half), full)
-        for k in range(max(lo, 1), hi):
+        for k in range(hi - 1, max(lo, 1) - 1, -1):
             ret_copy(k).start()
         if lo == 0:
             keep = pltpu.make_async_copy(outs.at[0], ret.at[0], load_sem.at[7])

time: 37.2 us -> 37.1 us (level)
  the two profiles are of different devices: /device:TPU:16 before, /device:TPU:11 now
where the time goes in v5:
time: 37.1 us; the launch traced here: 36.9 us
  Pallas kernels  36.9 us (99%)
    pallas_call x1, Pallas kernels, shards(): pl.pallas_call(functools.partial(kernel, n, full), out_shape=(jax.ShapeDt...  34.7 us
    pallas_call x1, Pallas kernels, shards(): pl.pallas_call(functools.partial(combine_kernel, full), out_shape=jax.Sha...  2.27 us

profile of v5, /device:TPU:11, one launch (start us, length us, event | category | flops | bytes accessed | tf_op | source)
XLA Modules:
  0.0 36.9 jit_solution(6908560101232280051)
XLA Ops:
  0.0 34.7 %shard_map.73 = (bf16[8,40,1024]{2,1,0:T(8,128)(2,1)}, bf16[2,128,192]{2,1,0:T(8,128)(2,1)}) custom-call(bf16[128,4096]{1,0:T(8,128)(2,1)} %tok_hbm.1, f32[1,4096]{1,0:T(1,128)} %bitcast.3, bf16[1,4096,384]{2,1,0:T(8,128)(2,1)} %gate_hbm.1, bf16[1,4096,384]{2,1,0:T(8,128)(2,1)} %up_hbm.1, bf16[1,384,4096]{2,1,0:T(8,128)(2,1)} %down_hbm.1, s32[8,20]{1,0:T(8,128)} %bitcast.4, ...), custom_call_target="tpu_custom_call" | custom-call | tf_op jit(solution)/shard_map/pallas_call | solution.py:257
  34.7 2.3 %shard_map.74 = bf16[128,2048]{1,0:T(8,128)(2,1)} custom-call(bf16[8,40,1024]{2,1,0:T(8,128)(2,1)} %get-tuple-element.7.ret_hbm, bf16[2,128,192]{2,1,0:T(8,128)(2,1)} %get-tuple-element.8.factors_hbm), custom_call_target="tpu_custom_call" | custom-call | tf_op jit(solution)/shard_map/pallas_call | solution.py:292
